TPU v7x, 32 devices: a whole 2x2x4 slice. The times are simulated.
32 devices in a mesh: rep: 2 (over x), fs: 8 (over z, y), tp: 2 (over core).
Axes of the slice: x: 2, y: 2, z: 4, core: 2. Of those that a mesh axis runs over, the one named last changes fastest.
Arguments:
- tokens: bfloat16 [4096, 2048], P(('rep', 'fs')), may hold values from -6 to 6
- ffn_gate: bfloat16 [2048, 5632], P('fs', 'tp'), may hold values from -0.125 to 0.125
- ffn_up: bfloat16 [2048, 5632], P('fs', 'tp'), may hold values from -0.125 to 0.125
- ffn_down: bfloat16 [5632, 2048], P('tp', 'fs'), may hold values from -0.3125 to 0.3125
- query_proj: bfloat16 [2048, 512], P('fs', 'tp'), may hold values from -0.125 to 0.125
- key_proj: bfloat16 [2048, 512], P('fs', 'tp'), may hold values from -0.125 to 0.125
- value_proj: bfloat16 [2048, 1024], P('fs', 'tp'), may hold values from -0.125 to 0.125
- outgate_proj: bfloat16 [2048, 1024], P('fs', 'tp'), may hold values from -0.125 to 0.125
- output_proj: bfloat16 [1024, 2048], P('tp', 'fs'), may hold values from -0.375 to 0.375
- rank_down: bfloat16 [2048, 16], replicated, may hold values from -0.1875 to 0.1875
- rank_up: bfloat16 [16, 512], replicated, may hold values from -3 to 3
- decay_bias: float32 [512], replicated, may hold values from -0.5 to 8
- head_gain: float32 [1024], replicated, may hold values from 0.1 to 1.9
- norm_gain: float32 [3, 2048], replicated, may hold values from 0.1 to 1.9
- norm_bias: float32 [3, 2048], replicated, may hold values from -2 to 2
Outputs:
- layer_out: bfloat16 [4096, 2048], P(('rep', 'fs'))
All inputs are finite; a program needn't handle non-finite values.
Results may differ from a plain program's by a relative error of at most 0.024.
Values may be sent and summed in bfloat16 or wider, within the bound.
No kernel may reach another device: no remote copies, remote signals or barrier semaphores. Data moves between devices by JAX's collectives and lax.ppermute only.
A program may use at most 128 MiB of HBM per device.

v0:
```python
import jax
import jax.numpy as jnp
from jax import lax
from jax.sharding import PartitionSpec as P

DK = 64
DV = 128
BLOCK = 64
EPSILON = 1e-05
HEAD_FLOOR = 1.0
RESIDUAL_SCALE = 2.0**0.5
GATE_SOFTNESS = 16.0
FULL_ACCURACY = lax.Precision.HIGHEST


def layer_norm(summed, norm_gain, norm_shift):
    centred = summed - jnp.mean(summed, -1, keepdims=True)
    spread = jnp.mean(centred * centred, -1, keepdims=True)
    return (centred * lax.rsqrt(spread + EPSILON) * norm_gain + norm_shift).astype(jnp.bfloat16)


def gla_heads(queries, keys_rows, values, decay_logarithm):
    length, head_count, key_width = queries.shape
    value_width = values.shape[-1]
    block_count = length // BLOCK

    def blocks(array):
        return array.reshape(block_count, BLOCK, head_count, array.shape[-1])

    causal = jnp.tril(jnp.ones((BLOCK, BLOCK), bool))[:, :, None, None]

    def advance(running_state, inputs):
        query_block, key_block, value_block, decay_blk = inputs
        decay_prefix = jnp.cumsum(decay_blk, axis=0)
        spread = decay_prefix[:, None] - decay_prefix[None, :]
        weight = jnp.exp(jnp.where(causal, spread, -jnp.inf))
        scores = jnp.einsum(
            "lshk,lhk,shk->hls", weight, query_block, key_block, precision=FULL_ACCURACY
        )
        within = jnp.einsum("hls,shv->lhv", scores, value_block, precision=FULL_ACCURACY)
        carried_over = jnp.einsum(
            "zew,ewa->zea",
            query_block * jnp.exp(decay_prefix),
            running_state,
            precision=FULL_ACCURACY,
        )
        block_finish = decay_prefix[-1]
        running_state = jnp.exp(block_finish)[:, :, None] * running_state + jnp.einsum(
            "oct,ocy->cty",
            key_block * jnp.exp(block_finish[None] - decay_prefix),
            value_block,
            precision=FULL_ACCURACY,
        )
        return (running_state, within + carried_over)

    initial = jnp.zeros((head_count, key_width, value_width), jnp.float32)
    _, outputs = lax.scan(
        advance,
        initial,
        (blocks(queries), blocks(keys_rows), blocks(values), blocks(decay_logarithm)),
    )
    return outputs.reshape(length, head_count, value_width)


def settle(partial_value, residual_rows, factor, norm_gain, norm_shift):
    summed = lax.psum(partial_value.astype(jnp.bfloat16), "tp").astype(jnp.float32)
    return layer_norm(
        RESIDUAL_SCALE * residual_rows.astype(jnp.float32) + factor * summed, norm_gain, norm_shift
    )


def channel_mix(normed, gate_full, up_full, down_full):
    gate_rows = jnp.dot(normed, gate_full, preferred_element_type=jnp.float32)
    up_rows = jnp.dot(normed, up_full, preferred_element_type=jnp.float32)
    hidden = (jax.nn.silu(gate_rows) * up_rows).astype(jnp.bfloat16)
    return jnp.dot(hidden, down_full, preferred_element_type=jnp.float32)


def per_device(
    tokens,
    ffn_gate,
    ffn_up,
    ffn_down,
    query_proj,
    key_proj,
    value_proj,
    outgate_proj,
    output_proj,
    rank_down,
    rank_up,
    decay_bias,
    head_gain,
    norm_gain,
    norm_bias,
):
    row_count = tokens.shape[0]
    gate_full, up_full = (
        lax.all_gather(ffn_gate, "fs", axis=0, tiled=True),
        lax.all_gather(ffn_up, "fs", axis=0, tiled=True),
    )
    down_full = lax.all_gather(ffn_down, "fs", axis=1, tiled=True)
    first_partial = channel_mix(tokens, gate_full, up_full, down_full)
    first = settle(first_partial, tokens, 0.5, norm_gain[0], norm_bias[0])
    key_cols = query_proj.shape[1]
    value_cols = value_proj.shape[1]
    query_full, key_full, value_full, outgate_full = (
        lax.all_gather(query_proj, "fs", axis=0, tiled=True),
        lax.all_gather(key_proj, "fs", axis=0, tiled=True),
        lax.all_gather(value_proj, "fs", axis=0, tiled=True),
        lax.all_gather(outgate_proj, "fs", axis=0, tiled=True),
    )
    joined_full = jnp.concatenate([query_full, key_full, value_full, outgate_full], axis=1)
    projected = jnp.dot(first, joined_full, preferred_element_type=jnp.float32)
    queries = projected[:, :key_cols] * DK ** (-0.5)
    keys_rows = projected[:, key_cols : 2 * key_cols]
    values = projected[:, 2 * key_cols : 2 * key_cols + value_cols]
    gates = projected[:, 2 * key_cols + value_cols :]
    head_count = key_cols // DK
    position = lax.axis_index("tp")
    key_start = position * (head_count * DK)
    value_start = position * (head_count * DV)
    rank_rows = jnp.dot(first, rank_down, preferred_element_type=jnp.float32)
    up_block = lax.dynamic_slice_in_dim(rank_up, key_start, head_count * DK, 1).astype(jnp.float32)
    bias_block = lax.dynamic_slice_in_dim(decay_bias, key_start, head_count * DK, 0)
    decay_source = jnp.dot(rank_rows, up_block, precision=FULL_ACCURACY) + bias_block
    decay_logarithm = jax.nn.log_sigmoid(decay_source) / GATE_SOFTNESS
    heads_out = gla_heads(
        queries.reshape(row_count, head_count, DK),
        keys_rows.reshape(row_count, head_count, DK),
        values.reshape(row_count, head_count, DV),
        decay_logarithm.reshape(row_count, head_count, DK),
    )
    scaled = heads_out * lax.rsqrt(jnp.mean(heads_out * heads_out, -1, keepdims=True) + HEAD_FLOOR)
    gain_block = lax.dynamic_slice_in_dim(head_gain, value_start, head_count * DV, 0)
    scaled = scaled * gain_block.reshape(head_count, DV)
    mixed = (scaled.reshape(row_count, head_count * DV) * jax.nn.silu(gates)).astype(jnp.bfloat16)
    mixer_partial = jnp.dot(
        mixed,
        lax.all_gather(output_proj, "fs", axis=1, tiled=True),
        preferred_element_type=jnp.float32,
    )
    second = settle(mixer_partial, first, 1.0, norm_gain[1], norm_bias[1])
    third_partial = channel_mix(second, gate_full, up_full, down_full)
    return settle(third_partial, second, 0.5, norm_gain[2], norm_bias[2])


def solution(mesh):
    return jax.shard_map(
        per_device,
        mesh=mesh,
        in_specs=(
            P(("rep", "fs"), None),
            P("fs", "tp"),
            P("fs", "tp"),
            P("tp", "fs"),
            P("fs", "tp"),
            P("fs", "tp"),
            P("fs", "tp"),
            P("fs", "tp"),
            P("tp", "fs"),
            P(),
            P(),
            P(),
            P(),
            P(),
            P(),
        ),
        out_specs=P(("rep", "fs"), None),
        check_vma=False,
    )
```

profile of v0, /device:TPU:0, one launch (start us, length us, event | category | flops | bytes accessed | tf_op | source)
XLA Modules:
  0.0 917.7 jit_solution(16187257873956331330)
XLA Ops:
  8.8 166.8 %all-gather.9.cloned.1.call-done = bf16[2048,2816]{1,0:T(8,128)(2,1)} async-done(((bf16[256,2816]{1,0:T(8,128)(2,1)}), bf16[2048,2816]{1,0:T(8,128)(2,1)}) %all-gather.9.cloned.1.call-update) | async-done | bytes 11534352 | tf_op jit(solution)/shard_map/all_gather | solution.py:98
  175.6 9.0 fusion.50
  184.6 154.7 %all-gather.11.cloned.1.call-done = bf16[2048,2816]{1,0:T(8,128)(2,1)} async-done(((bf16[256,2816]{1,0:T(8,128)(2,1)}), bf16[2048,2816]{1,0:T(8,128)(2,1)}) %all-gather.11.cloned.1.call-update) | async-done | bytes 11534352 | tf_op jit(solution)/shard_map/all_gather | solution.py:99
  339.3 163.6 %all-gather.13.cloned.1.call-done = bf16[2816,2048]{1,0:T(8,128)(2,1)} async-done(((bf16[2816,256]{1,0:T(8,128)(2,1)}), bf16[2816,2048]{1,0:T(8,128)(2,1)}) %all-gather.13.cloned.1.call-update) | async-done | bytes 11534352 | tf_op jit(solution)/shard_map/all_gather | solution.py:101
  502.9 15.5 %convolution_convert_fusion.2 = bf16[256,2048]{1,0:T(8,128)(2,1)} fusion(bf16[2816,2048]{1,0:T(8,128)(2,1)} %all-gather.13.cloned.1.call-done, bf16[256,2048]{1,0:T(8,128)(2,1)S(1)} %copy-done.2, bf16[2048,2816]{1,0:T(8,128)(2,1)} %all-gather.11.cloned.1.call-done, f32[256,2816]{1,0:T(8,128)} %fusion.50), kind=kOutput, calls=%fused_computation.45 | convolution fusion | flops 5910429696 | bytes 28049408 | tf_op jit(solution)/shard_map/dot_general | solution.py:76
  521.9 14.4 %all-reduce.6.cloned.1.call-start = ((), (), s32[]{:S(2)}) async-start(), calls=%async_computation.9 | async-start | bytes 2097152 | tf_op jit(solution)/shard_map/psum | solution.py:66
  539.7 40.0 %all-gather.15.cloned.1.call-done = bf16[2048,256]{1,0:T(8,128)(2,1)} async-done(((bf16[256,256]{1,0:T(8,128)(2,1)}), bf16[2048,256]{1,0:T(8,128)(2,1)}) %all-gather.15.cloned.1.call-update) | async-done | bytes 1048592 | tf_op jit(solution)/shard_map/all_gather | solution.py:107
  579.7 41.0 %all-gather.17.cloned.1.call-done = bf16[2048,256]{1,0:T(8,128)(2,1)} async-done(((bf16[256,256]{1,0:T(8,128)(2,1)}), bf16[2048,256]{1,0:T(8,128)(2,1)}) %all-gather.17.cloned.1.call-update) | async-done | bytes 1048592 | tf_op jit(solution)/shard_map/all_gather | solution.py:108
  620.7 50.0 %all-gather.19.cloned.1.call-done = bf16[2048,512]{1,0:T(8,128)(2,1)} async-done(((bf16[256,512]{1,0:T(8,128)(2,1)}), bf16[2048,512]{1,0:T(8,128)(2,1)}) %all-gather.19.cloned.1.call-update) | async-done | bytes 2097168 | tf_op jit(solution)/shard_map/all_gather | solution.py:109
  670.7 49.8 %all-gather.21.cloned.1.call-done = bf16[2048,512]{1,0:T(8,128)(2,1)} async-done(((bf16[256,512]{1,0:T(8,128)(2,1)}), bf16[2048,512]{1,0:T(8,128)(2,1)}) %all-gather.21.cloned.1.call-update) | async-done | bytes 2097168 | tf_op jit(solution)/shard_map/all_gather | solution.py:110
  720.4 3.9 fusion.20
  727.7 105.8 %while.13 = (s32[]{:T(128)}, f32[4,64,128]{2,1,0:T(8,128)S(1)}, f32[4,64,4,128]{3,1,2,0:T(8,128)}, f32[4,64,4,64]{3,2,1,0:T(4,128)S(1)}, f32[4,64,4,64]{3,2,1,0:...) while((s32[]{:T(128)}, f32[4,64,128]{2,1,0:T(8,128)S(1)}, ...), condition=%wide.region_5.6_spmd.clone, body=%wide.region_3.5_spmd.clone.sunk | while | flops 92475392 | bytes 10893944 | solution.py:57
  728.8 5.9 multiply_bitcast_fusion.2
  734.7 17.6 %fusion.91 = f32[4,64,1,64]{3,2,1,0:T(1,128)S(1)} fusion(f32[64,4,64,64]{2,1,3,0:T(4,128)S(1)} %multiply_bitcast_fusion.2, f32[64,4,64,1]{2,1,0,3:T(4,128)S(1)} %dynamic-slice_bitcast_fusion.4), kind=kOutput, calls=%fused_computation.1.clone.1 | convolution fusion | flops 12582912 | bytes 4325376 | tf_op jit(solution)/shard_map/while/body/eval_jaxpr/lshk,lhk,shk->hls/dot_general | solution.py:37
  755.2 5.9 multiply_bitcast_fusion.2
  761.1 17.6 %fusion.91 = f32[4,64,1,64]{3,2,1,0:T(1,128)S(1)} fusion(f32[64,4,64,64]{2,1,3,0:T(4,128)S(1)} %multiply_bitcast_fusion.2, f32[64,4,64,1]{2,1,0,3:T(4,128)S(1)} %dynamic-slice_bitcast_fusion.4), kind=kOutput, calls=%fused_computation.1.clone.1 | convolution fusion | flops 12582912 | bytes 4325376 | tf_op jit(solution)/shard_map/while/body/eval_jaxpr/lshk,lhk,shk->hls/dot_general | solution.py:37
  781.6 5.9 multiply_bitcast_fusion.2
  787.5 17.6 %fusion.91 = f32[4,64,1,64]{3,2,1,0:T(1,128)S(1)} fusion(f32[64,4,64,64]{2,1,3,0:T(4,128)S(1)} %multiply_bitcast_fusion.2, f32[64,4,64,1]{2,1,0,3:T(4,128)S(1)} %dynamic-slice_bitcast_fusion.4), kind=kOutput, calls=%fused_computation.1.clone.1 | convolution fusion | flops 12582912 | bytes 4325376 | tf_op jit(solution)/shard_map/while/body/eval_jaxpr/lshk,lhk,shk->hls/dot_general | solution.py:37
  808.0 5.9 multiply_bitcast_fusion.2
  813.9 17.6 %fusion.91 = f32[4,64,1,64]{3,2,1,0:T(1,128)S(1)} fusion(f32[64,4,64,64]{2,1,3,0:T(4,128)S(1)} %multiply_bitcast_fusion.2, f32[64,4,64,1]{2,1,0,3:T(4,128)S(1)} %dynamic-slice_bitcast_fusion.4), kind=kOutput, calls=%fused_computation.1.clone.1 | convolution fusion | flops 12582912 | bytes 4325376 | tf_op jit(solution)/shard_map/while/body/eval_jaxpr/lshk,lhk,shk->hls/dot_general | solution.py:37
  840.2 18.1 %all-reduce.6.cloned.1.call-done = bf16[256,2048]{1,0:T(8,128)(2,1)} async-done(((bf16[256,2048]{1,0:T(8,128)(2,1)}), bf16[256,2048]{1,0:T(8,128)(2,1)}) %all-reduce.6.cloned.1.call-update) | async-done | bytes 1048592 | tf_op jit(solution)/shard_map/psum | solution.py:66
  861.2 9.0 fusion.52
  870.3 15.5 %convolution_convert_fusion = bf16[256,2048]{1,0:T(8,128)(2,1)} fusion(bf16[2816,2048]{1,0:T(8,128)(2,1)} %all-gather.13.cloned.1.call-done, bf16[256,2048]{1,0:T(8,128)(2,1)S(1)} %add_convert_fusion.1, bf16[2048,2816]{1,0:T(8,128)(2,1)} %all-gather.11.cloned.1.call-done, f32[256,2816]{1,0:T(8,128)} %fusion.52), kind=kOutput, calls=%fused_computation.43 | convolution fusion | flops 5910429696 | bytes 28049408 | tf_op jit(solution)/shard_map/dot_general | solution.py:76
  885.9 20.8 %all-reduce.8.cloned.1.call-done = bf16[256,2048]{1,0:T(8,128)(2,1)} async-done(((bf16[256,2048]{1,0:T(8,128)(2,1)}), bf16[256,2048]{1,0:T(8,128)(2,1)}) %all-reduce.8.cloned.1.call-update) | async-done | bytes 1048592 | tf_op jit(solution)/shard_map/psum | solution.py:66
  (123 shorter events, 37.4 us)
Async XLA Ops:
  6.5 717.8 %copy-start = (bf16[2048,16]{0,1:T(8,128)(2,1)S(1)}, bf16[2048,16]{0,1:T(8,128)(2,1)}, u32[]{:S(2)}) copy-start(bf16[2048,16]{0,1:T(8,128)(2,1)} %param.26) | copy-start | bytes 196612
  6.5 169.1 %copy-start.2 = (bf16[256,2048]{1,0:T(8,128)(2,1)S(1)}, bf16[256,2048]{1,0:T(8,128)(2,1)}, u32[]{:S(2)}) copy-start(bf16[256,2048]{1,0:T(8,128)(2,1)} %param.17) | copy-start | bytes 3145732
  6.5 169.1 %all-gather.9.cloned.1.call-start = ((), (), s32[]{:S(2)}) async-start(), calls=%async_computation | async-start | bytes 12976128 | tf_op jit(solution)/shard_map/all_gather | solution.py:98
  7.3 332.0 %all-gather.11.cloned.1.call-start = ((), (), s32[]{:S(2)}) async-start(), calls=%async_computation.1 | async-start | bytes 12976128 | tf_op jit(solution)/shard_map/all_gather | solution.py:99
  8.0 494.9 %all-gather.13.cloned.1.call-start = ((), (), s32[]{:S(2)}) async-start(), calls=%async_computation.2 | async-start | bytes 12976128 | tf_op jit(solution)/shard_map/all_gather | solution.py:101
  8.7 527.8 %all-reduce.4.cloned.1.call-start = ((), (), s32[]{:S(2)}) async-start(), calls=%async_computation.3 | async-start | bytes 2097152 | tf_op jit(solution)/shard_map/psum | solution.py:66
  518.4 17.9 %copy-start.7 = (f32[3,2048]{1,0:T(4,128)S(1)}, f32[3,2048]{1,0:T(4,128)}, u32[]{:S(2)}) copy-start(f32[3,2048]{1,0:T(4,128)} %param.30) | copy-start | bytes 73732
  518.4 17.9 %copy-start.8 = (f32[3,2048]{1,0:T(4,128)S(1)}, f32[3,2048]{1,0:T(4,128)}, u32[]{:S(2)}) copy-start(f32[3,2048]{1,0:T(4,128)} %param.31) | copy-start | bytes 73732
  518.4 18.0 %copy-start.10 = (f32[512]{0:T(512)S(1)}, f32[512]{0:T(512)}, u32[]{:S(2)}) copy-start(f32[512]{0:T(512)} %param.28) | copy-start | bytes 6148
  518.4 18.0 %copy-start.9 = (f32[1024]{0:T(1024)S(1)}, f32[1024]{0:T(1024)}, u32[]{:S(2)}) copy-start(f32[1024]{0:T(1024)} %param.29) | copy-start | bytes 12292
  518.5 61.2 %all-gather.15.cloned.1.call-start = ((), (), s32[]{:S(2)}) async-start(), calls=%async_computation.4 | async-start | bytes 1179648 | tf_op jit(solution)/shard_map/all_gather | solution.py:107
  519.1 101.6 %all-gather.17.cloned.1.call-start = ((), (), s32[]{:S(2)}) async-start(), calls=%async_computation.5 | async-start | bytes 1179648 | tf_op jit(solution)/shard_map/all_gather | solution.py:108
  519.6 151.0 %all-gather.19.cloned.1.call-start = ((), (), s32[]{:S(2)}) async-start(), calls=%async_computation.6 | async-start | bytes 2359296 | tf_op jit(solution)/shard_map/all_gather | solution.py:109
  520.4 200.0 %all-gather.21.cloned.1.call-start = ((), (), s32[]{:S(2)}) async-start(), calls=%async_computation.7 | async-start | bytes 2359296 | tf_op jit(solution)/shard_map/all_gather | solution.py:110
  521.1 315.2 %all-gather.23.cloned.1.call-start = ((), (), s32[]{:S(2)}) async-start(), calls=%async_computation.8 | async-start | bytes 2359296 | tf_op jit(solution)/shard_map/all_gather | solution.py:139
  521.9 336.4 %all-reduce.6.cloned.1.call-start = ((), (), s32[]{:S(2)}) async-start(), calls=%async_computation.9 | async-start | bytes 2097152 | tf_op jit(solution)/shard_map/psum | solution.py:66
  536.6 1.8 copy-start.3
  724.3 1.2 copy-start.6
  724.3 1.2 copy-start.11
  726.0 1.5 slice-start
  840.2 66.5 %all-reduce.8.cloned.1.call-start = ((), (), s32[]{:S(2)}) async-start(), calls=%async_computation.10 | async-start | bytes 2097152 | tf_op jit(solution)/shard_map/psum | solution.py:66
  858.3 1.7 copy-start.4
  906.6 1.8 copy-start.5
  908.4 2.3 copy-start.1
Sparse Core Ops, SparseCore 0:
  9.5 166.0 all-gather.8
  177.8 161.4 all-gather.10
  341.4 161.4 all-gather.12
  518.6 17.5 all-reduce.3
  538.2 41.4 all-gather.14
  581.7 38.9 all-gather.16
  622.8 47.7 all-gather.18
  672.8 47.6 all-gather.20
  722.5 48.7 all-gather.22
  840.3 17.9 all-reduce.5
  886.0 20.5 all-reduce.7
where the time goes:
time: 924 us; the launch traced here: 918 us
  waiting for transfers between devices  710 us (77%)
  matrix products  135 us (15%)
  other arithmetic  39.5 us (4%)
  starting transfers between devices  14.8 us (2%)
  between operations  13.8 us (1%)
    all_gather x1, waiting for transfers between devices, per_device(): lax.all_gather(ffn_gate, 'fs', axis=0, tiled=True)  167 us
    all_gather x1, waiting for transfers between devices, per_device(): down_full = lax.all_gather(ffn_down, 'fs', axis=1, tiled=True)  164 us
    all_gather x1, waiting for transfers between devices, per_device(): lax.all_gather(ffn_up, 'fs', axis=0, tiled=True)  155 us
    dot_general x4, matrix products, advance(): jnp.einsum('lshk,lhk,shk->hls', weight, query_block, key_block, precision...  70.4 us
    all_gather x1, waiting for transfers between devices, per_device(): lax.all_gather(value_proj, 'fs', axis=0, tiled=True)  50 us
    all_gather x1, waiting for transfers between devices, per_device(): lax.all_gather(outgate_proj, 'fs', axis=0, tiled=True)  49.8 us
    all_gather x1, waiting for transfers between devices, per_device(): lax.all_gather(key_proj, 'fs', axis=0, tiled=True)  41 us
    all_gather x1, waiting for transfers between devices, per_device(): lax.all_gather(query_proj, 'fs', axis=0, tiled=True)  40 us
  transfers between devices with their start and end apart: 11, of which 9 were waited for; matrix products, arithmetic and copies ran while one was open for 14% of the time, Pallas kernels for 0%

commit v1 on v0

--- a/solution.py
+++ b/solution.py
@@ -98,7 +98,7 @@
         lax.all_gather(ffn_gate, "fs", axis=0, tiled=True),
         lax.all_gather(ffn_up, "fs", axis=0, tiled=True),
     )
-    down_full = lax.all_gather(ffn_down, "fs", axis=1, tiled=True)
+    down_full = jnp.concatenate(lax.all_gather(ffn_down, "fs"), axis=1)
     first_partial = channel_mix(tokens, gate_full, up_full, down_full)
     first = settle(first_partial, tokens, 0.5, norm_gain[0], norm_bias[0])
     key_cols = query_proj.shape[1]

time: 924 us -> 929 us (level)
  local copies, waits for them, and re-layouts: 4.66 us -> 24.7 us
  waiting for transfers between devices: 710 us -> 695 us
    all_gather x1, waiting for transfers between devices: 167 us -> 148 us  [per_device(): lax.all_gather(ffn_gate, 'fs', axis=0, tiled=True)]
    reshape x0 -> x1, local copies, waits for them, and re-layouts: none -> 15.5 us  [per_device(): down_full = jnp.concatenate(lax.all_gather(ffn_down, 'fs'), axis=1)]
  transfers between devices with their start and end apart: 11 -> 11, of which waited for: 9 -> 9; matrix products, arithmetic and copies ran while one was open for 14% -> 16% of each run, Pallas kernels for 0% -> 0%
where the time goes in v1:
time: 929 us; the launch traced here: 922 us
  waiting for transfers between devices  695 us (75%)
  matrix products  134 us (14%)
  other arithmetic  39.5 us (4%)
  local copies, waits for them, and re-layouts  24.7 us (3%)
  starting transfers between devices  14.8 us (2%)
  between operations  13.9 us (1%)
    all_gather x1, waiting for transfers between devices, per_device(): down_full = jnp.concatenate(lax.all_gather(ffn_down, 'fs'), axis=1)  167 us
    all_gather x1, waiting for transfers between devices, per_device(): lax.all_gather(ffn_up, 'fs', axis=0, tiled=True)  155 us
    all_gather x1, waiting for transfers between devices, per_device(): lax.all_gather(ffn_gate, 'fs', axis=0, tiled=True)  148 us
    dot_general x4, matrix products, advance(): jnp.einsum('lshk,lhk,shk->hls', weight, query_block, key_block, precision...  70.4 us
    all_gather x1, waiting for transfers between devices, per_device(): lax.all_gather(value_proj, 'fs', axis=0, tiled=True)  50 us
    all_gather x1, waiting for transfers between devices, per_device(): lax.all_gather(outgate_proj, 'fs', axis=0, tiled=True)  49.8 us
    all_gather x1, waiting for transfers between devices, per_device(): lax.all_gather(key_proj, 'fs', axis=0, tiled=True)  41 us
    all_gather x1, waiting for transfers between devices, per_device(): lax.all_gather(query_proj, 'fs', axis=0, tiled=True)  40 us
  transfers between devices with their start and end apart: 11, of which 9 were waited for; matrix products, arithmetic and copies ran while one was open for 16% of the time, Pallas kernels for 0%

profile of v1, /device:TPU:0, one launch (start us, length us, event | category | flops | bytes accessed | tf_op | source)
XLA Modules:
  0.0 922.2 jit_solution(5175220783456150271)
XLA Ops:
  8.8 166.8 %all-gather.24.cloned.1.call-done = bf16[22528,256]{1,0:T(8,128)(2,1)} async-done(((bf16[2816,256]{1,0:T(8,128)(2,1)}), bf16[22528,256]{1,0:T(8,128)(2,1)}) %all-gather.24.cloned.1.call-update) | async-done | bytes 11534352 | tf_op jit(solution)/shard_map/all_gather | solution.py:101
  175.6 15.5 %copy.36 = bf16[2816,8,256]{0,2,1:T(8,128)(2,1)} copy(bf16[2816,8,256]{2,0,1:T(8,128)(2,1)} %bitcast.109) | data formatting | bytes 23068672 | tf_op jit(solution)/shard_map/reshape | solution.py:101
  191.1 148.2 %all-gather.10.cloned.1.call-done = bf16[2048,2816]{1,0:T(8,128)(2,1)} async-done(((bf16[256,2816]{1,0:T(8,128)(2,1)}), bf16[2048,2816]{1,0:T(8,128)(2,1)}) %all-gather.10.cloned.1.call-update) | async-done | bytes 11534352 | tf_op jit(solution)/shard_map/all_gather | solution.py:98
  339.3 9.0 fusion.50
  348.3 154.7 %all-gather.12.cloned.1.call-done = bf16[2048,2816]{1,0:T(8,128)(2,1)} async-done(((bf16[256,2816]{1,0:T(8,128)(2,1)}), bf16[2048,2816]{1,0:T(8,128)(2,1)}) %all-gather.12.cloned.1.call-update) | async-done | bytes 11534352 | tf_op jit(solution)/shard_map/all_gather | solution.py:99
  503.0 15.5 %convolution_convert_fusion.2 = bf16[256,2048]{1,0:T(8,128)(2,1)} fusion(bf16[2816,2048]{0,1:T(8,128)(2,1)} %bitcast.107, bf16[256,2048]{1,0:T(8,128)(2,1)S(1)} %copy-done.2, bf16[2048,2816]{1,0:T(8,128)(2,1)} %all-gather.12.cloned.1.call-done, f32[256,2816]{1,0:T(8,128)} %fusion.50), kind=kOutput, calls=%fused_computation.45 | convolution fusion | flops 5910429696 | bytes 28049408 | tf_op jit(solution)/shard_map/dot_general | solution.py:76
  522.0 14.4 %all-reduce.6.cloned.1.call-start = ((), (), s32[]{:S(2)}) async-start(), calls=%async_computation.8 | async-start | bytes 2097152 | tf_op jit(solution)/shard_map/psum | solution.py:66
  539.8 40.0 %all-gather.14.cloned.1.call-done = bf16[2048,256]{1,0:T(8,128)(2,1)} async-done(((bf16[256,256]{1,0:T(8,128)(2,1)}), bf16[2048,256]{1,0:T(8,128)(2,1)}) %all-gather.14.cloned.1.call-update) | async-done | bytes 1048592 | tf_op jit(solution)/shard_map/all_gather | solution.py:107
  579.8 41.0 %all-gather.16.cloned.1.call-done = bf16[2048,256]{1,0:T(8,128)(2,1)} async-done(((bf16[256,256]{1,0:T(8,128)(2,1)}), bf16[2048,256]{1,0:T(8,128)(2,1)}) %all-gather.16.cloned.1.call-update) | async-done | bytes 1048592 | tf_op jit(solution)/shard_map/all_gather | solution.py:108
  620.8 50.0 %all-gather.18.cloned.1.call-done = bf16[2048,512]{1,0:T(8,128)(2,1)} async-done(((bf16[256,512]{1,0:T(8,128)(2,1)}), bf16[2048,512]{1,0:T(8,128)(2,1)}) %all-gather.18.cloned.1.call-update) | async-done | bytes 2097168 | tf_op jit(solution)/shard_map/all_gather | solution.py:109
  670.8 49.8 %all-gather.20.cloned.1.call-done = bf16[2048,512]{1,0:T(8,128)(2,1)} async-done(((bf16[256,512]{1,0:T(8,128)(2,1)}), bf16[2048,512]{1,0:T(8,128)(2,1)}) %all-gather.20.cloned.1.call-update) | async-done | bytes 2097168 | tf_op jit(solution)/shard_map/all_gather | solution.py:110
  728.7 109.4 %while.13 = (s32[]{:T(128)}, f32[4,64,128]{2,1,0:T(8,128)S(1)}, f32[4,64,4,128]{3,1,2,0:T(8,128)}, f32[4,64,4,64]{3,2,1,0:T(4,128)S(1)}, f32[4,64,4,64]{3,2,1,0:...) while((s32[]{:T(128)}, f32[4,64,128]{2,1,0:T(8,128)S(1)}, ...), condition=%wide.region_5.6_spmd.clone, body=%wide.region_3.5_spmd.clone.sunk | while | flops 92475392 | bytes 10893944 | solution.py:57
  729.8 5.9 multiply_bitcast_fusion.2
  735.7 17.6 %fusion.91 = f32[4,64,1,64]{3,2,1,0:T(1,128)S(1)} fusion(f32[64,4,64,64]{2,1,3,0:T(4,128)S(1)} %multiply_bitcast_fusion.2, f32[64,4,64,1]{2,1,0,3:T(4,128)S(1)} %dynamic-slice_bitcast_fusion.4), kind=kOutput, calls=%fused_computation.1.clone.1 | convolution fusion | flops 12582912 | bytes 4325376 | tf_op jit(solution)/shard_map/while/body/eval_jaxpr/lshk,lhk,shk->hls/dot_general | solution.py:37
  757.1 5.9 multiply_bitcast_fusion.2
  763.0 17.6 %fusion.91 = f32[4,64,1,64]{3,2,1,0:T(1,128)S(1)} fusion(f32[64,4,64,64]{2,1,3,0:T(4,128)S(1)} %multiply_bitcast_fusion.2, f32[64,4,64,1]{2,1,0,3:T(4,128)S(1)} %dynamic-slice_bitcast_fusion.4), kind=kOutput, calls=%fused_computation.1.clone.1 | convolution fusion | flops 12582912 | bytes 4325376 | tf_op jit(solution)/shard_map/while/body/eval_jaxpr/lshk,lhk,shk->hls/dot_general | solution.py:37
  784.4 5.9 multiply_bitcast_fusion.2
  790.3 17.6 %fusion.91 = f32[4,64,1,64]{3,2,1,0:T(1,128)S(1)} fusion(f32[64,4,64,64]{2,1,3,0:T(4,128)S(1)} %multiply_bitcast_fusion.2, f32[64,4,64,1]{2,1,0,3:T(4,128)S(1)} %dynamic-slice_bitcast_fusion.4), kind=kOutput, calls=%fused_computation.1.clone.1 | convolution fusion | flops 12582912 | bytes 4325376 | tf_op jit(solution)/shard_map/while/body/eval_jaxpr/lshk,lhk,shk->hls/dot_general | solution.py:37
  811.7 5.9 multiply_bitcast_fusion.2
  817.6 17.6 %fusion.91 = f32[4,64,1,64]{3,2,1,0:T(1,128)S(1)} fusion(f32[64,4,64,64]{2,1,3,0:T(4,128)S(1)} %multiply_bitcast_fusion.2, f32[64,4,64,1]{2,1,0,3:T(4,128)S(1)} %dynamic-slice_bitcast_fusion.4), kind=kOutput, calls=%fused_computation.1.clone.1 | convolution fusion | flops 12582912 | bytes 4325376 | tf_op jit(solution)/shard_map/while/body/eval_jaxpr/lshk,lhk,shk->hls/dot_general | solution.py:37
  844.7 18.1 %all-reduce.6.cloned.1.call-done = bf16[256,2048]{1,0:T(8,128)(2,1)} async-done(((bf16[256,2048]{1,0:T(8,128)(2,1)}), bf16[256,2048]{1,0:T(8,128)(2,1)}) %all-reduce.6.cloned.1.call-update) | async-done | bytes 1048592 | tf_op jit(solution)/shard_map/psum | solution.py:66
  865.7 9.0 fusion.52
  874.8 15.5 %convolution_convert_fusion = bf16[256,2048]{1,0:T(8,128)(2,1)} fusion(bf16[2816,2048]{0,1:T(8,128)(2,1)} %bitcast.108, bf16[256,2048]{1,0:T(8,128)(2,1)S(1)} %add_convert_fusion.1, bf16[2048,2816]{1,0:T(8,128)(2,1)} %all-gather.12.cloned.1.call-done, f32[256,2816]{1,0:T(8,128)} %fusion.52), kind=kOutput, calls=%fused_computation.43 | convolution fusion | flops 5910429696 | bytes 28049408 | tf_op jit(solution)/shard_map/dot_general | solution.py:76
  890.4 20.8 %all-reduce.8.cloned.1.call-done = bf16[256,2048]{1,0:T(8,128)(2,1)} async-done(((bf16[256,2048]{1,0:T(8,128)(2,1)}), bf16[256,2048]{1,0:T(8,128)(2,1)}) %all-reduce.8.cloned.1.call-update) | async-done | bytes 1048592 | tf_op jit(solution)/shard_map/psum | solution.py:66
  (126 shorter events, 45.6 us)
Async XLA Ops:
  6.5 718.0 %copy-start = (bf16[2048,16]{0,1:T(8,128)(2,1)S(1)}, bf16[2048,16]{0,1:T(8,128)(2,1)}, u32[]{:S(2)}) copy-start(bf16[2048,16]{0,1:T(8,128)(2,1)} %param.26) | copy-start | bytes 196612
  6.5 169.1 %all-gather.24.cloned.1.call-start = ((), (), s32[]{:S(2)}) async-start(), calls=%async_computation.10 | async-start | bytes 12976128 | tf_op jit(solution)/shard_map/all_gather | solution.py:101
  7.3 332.0 %all-gather.10.cloned.1.call-start = ((), (), s32[]{:S(2)}) async-start(), calls=%async_computation | async-start | bytes 12976128 | tf_op jit(solution)/shard_map/all_gather | solution.py:98
  8.0 495.0 %all-gather.12.cloned.1.call-start = ((), (), s32[]{:S(2)}) async-start(), calls=%async_computation.1 | async-start | bytes 12976128 | tf_op jit(solution)/shard_map/all_gather | solution.py:99
  8.7 527.9 %all-reduce.4.cloned.1.call-start = ((), (), s32[]{:S(2)}) async-start(), calls=%async_computation.2 | async-start | bytes 2097152 | tf_op jit(solution)/shard_map/psum | solution.py:66
  175.6 163.7 %copy-start.2 = (bf16[256,2048]{1,0:T(8,128)(2,1)S(1)}, bf16[256,2048]{1,0:T(8,128)(2,1)}, u32[]{:S(2)}) copy-start(bf16[256,2048]{1,0:T(8,128)(2,1)} %param.17) | copy-start | bytes 3145732
  518.6 17.9 %copy-start.8 = (f32[3,2048]{1,0:T(4,128)S(1)}, f32[3,2048]{1,0:T(4,128)}, u32[]{:S(2)}) copy-start(f32[3,2048]{1,0:T(4,128)} %param.30) | copy-start | bytes 73732
  518.6 17.9 %copy-start.9 = (f32[3,2048]{1,0:T(4,128)S(1)}, f32[3,2048]{1,0:T(4,128)}, u32[]{:S(2)}) copy-start(f32[3,2048]{1,0:T(4,128)} %param.31) | copy-start | bytes 73732
  518.6 18.0 %copy-start.11 = (f32[512]{0:T(512)S(1)}, f32[512]{0:T(512)}, u32[]{:S(2)}) copy-start(f32[512]{0:T(512)} %param.28) | copy-start | bytes 6148
  518.6 18.0 %copy-start.10 = (f32[1024]{0:T(1024)S(1)}, f32[1024]{0:T(1024)}, u32[]{:S(2)}) copy-start(f32[1024]{0:T(1024)} %param.29) | copy-start | bytes 12292
  518.6 61.2 %all-gather.14.cloned.1.call-start = ((), (), s32[]{:S(2)}) async-start(), calls=%async_computation.3 | async-start | bytes 1179648 | tf_op jit(solution)/shard_map/all_gather | solution.py:107
  519.2 101.7 %all-gather.16.cloned.1.call-start = ((), (), s32[]{:S(2)}) async-start(), calls=%async_computation.4 | async-start | bytes 1179648 | tf_op jit(solution)/shard_map/all_gather | solution.py:108
  519.8 151.0 %all-gather.18.cloned.1.call-start = ((), (), s32[]{:S(2)}) async-start(), calls=%async_computation.5 | async-start | bytes 2359296 | tf_op jit(solution)/shard_map/all_gather | solution.py:109
  520.5 200.1 %all-gather.20.cloned.1.call-start = ((), (), s32[]{:S(2)}) async-start(), calls=%async_computation.6 | async-start | bytes 2359296 | tf_op jit(solution)/shard_map/all_gather | solution.py:110
  521.3 319.7 %all-gather.22.cloned.1.call-start = ((), (), s32[]{:S(2)}) async-start(), calls=%async_computation.7 | async-start | bytes 2359296 | tf_op jit(solution)/shard_map/all_gather | solution.py:139
  522.0 340.8 %all-reduce.6.cloned.1.call-start = ((), (), s32[]{:S(2)}) async-start(), calls=%async_computation.8 | async-start | bytes 2097152 | tf_op jit(solution)/shard_map/psum | solution.py:66
  536.7 1.8 copy-start.3
  724.5 1.2 copy-start.6
  726.1 1.6 slice-start
  838.0 3.3 copy-start.7
  844.7 66.5 %all-reduce.8.cloned.1.call-start = ((), (), s32[]{:S(2)}) async-start(), calls=%async_computation.9 | async-start | bytes 2097152 | tf_op jit(solution)/shard_map/psum | solution.py:66
  862.8 1.7 copy-start.4
  911.1 1.8 copy-start.5
  912.9 2.3 copy-start.1
  (1 other events, 1.2 us)
Sparse Core Ops, SparseCore 0:
  9.5 166.0 all-gather.23
  177.8 161.4 all-gather.9
  341.5 161.4 all-gather.11
  518.7 17.6 all-reduce.3
  538.3 41.4 all-gather.13
  581.8 38.9 all-gather.15
  623.0 47.7 all-gather.17
  672.9 47.6 all-gather.19
  722.6 48.8 all-gather.21
  844.8 17.9 all-reduce.5
  890.5 20.5 all-reduce.7
